TPU v7x, 512 devices: a whole 4x8x8 slice. The times are simulated.
512 devices in a mesh: ep: 128 (over z, y, core), tp: 4 (over x).
Axes of the slice: x: 4, y: 8, z: 8, core: 2. Of those that a mesh axis runs over, the one named last changes fastest.
Arguments:
- tokens: bfloat16 [2048, 1024], P(('ep', 'tp')), may hold values from -6 to 6
- lengths: int32 [2048], P('ep'), may hold values from 256 to 1024
- key_cache: bfloat16 [2048, 1024, 128], P(('ep', 'tp')), may hold values from -1500 to 1500
- value_cache: bfloat16 [2048, 1024, 128], P(('ep', 'tp')), may hold values from -6 to 6
- query_weight: bfloat16 [1024, 512], P(None, 'tp'), may hold values from -0.1875 to 0.1875
- key_weight: bfloat16 [1024, 128], replicated, may hold values from -0.1875 to 0.1875
- value_weight: bfloat16 [1024, 128], replicated, may hold values from -0.1875 to 0.1875
- lambdas: float32 [4], replicated, may hold values from 0.3 to 0.8
- head_gain: float32 [128], replicated, may hold values from 0.1 to 1.9
- output_weight: bfloat16 [512, 1024], P(None, 'tp'), may hold values from -0.25 to 0.25
- norm1_gain: float32 [1024], replicated, may hold values from 0.1 to 1.9
- routes: int32 [2048, 6], P('ep'), may hold values from 0 to 127, all different within a row; in each aligned block of 16 rows (0 to 15, 16 to 31, ...) at most 2 rows name the same one
- route_logits: float32 [2048, 6], P('ep'), may hold values from -9 to 410
- gate_weight: bfloat16 [128, 1024, 1024], P('ep', None, 'tp'), may hold values from -0.5 to 0.5
- up_weight: bfloat16 [128, 1024, 1024], P('ep', None, 'tp'), may hold values from -0.5 to 0.5
- down_weight: bfloat16 [128, 1024, 1024], P('ep', 'tp'), may hold values from -0.09375 to 0.09375
- norm2_gain: float32 [1024], replicated, may hold values from 0.1 to 1.9
Outputs:
- mixed: bfloat16 [2048, 1024], P('ep', 'tp')
Inputs may be any that keep to these rules, and one draw needn't show every extreme that they name: `routes`: in the 16 rows of each aligned block (the rows held by one index of ep) no expert is named by more than 2 rows, a bound that some block reaches; the experts of a row differ.
All inputs are finite; a program needn't handle non-finite values.
Results may differ from a plain program's by a relative error of at most 0.014.
Values may be sent and summed in bfloat16 or wider, within the bound.
A program may use at most 64 MiB of HBM per device.

v0:
```python
import jax
import jax.numpy as jnp
from jax import lax
from jax.sharding import PartitionSpec as P

ALPHA = 1.4142135623730951
EPS = 1e-05
THETA = 500000.0
LIMIT = 7.0
SLOPE = 1.702


def copy_for_each(x, axis):
    count = lax.axis_size(axis)
    return lax.all_to_all(jnp.broadcast_to(x[None], (count, *x.shape)), axis, 0, 0, tiled=True)


def in_order(pieces, dim):
    lengths = list(pieces.shape[1:])
    lengths[dim] *= pieces.shape[0]
    return jnp.moveaxis(pieces, 0, dim).reshape(lengths)


def gathered_copies(x, axis, dim):
    pieces = copy_for_each(x, axis)
    return in_order(pieces, dim)


def split_up(x, dim, count):
    lengths = x.shape
    pieces = x.reshape(*lengths[:dim], count, lengths[dim] // count, *lengths[dim + 1 :])
    return jnp.moveaxis(pieces, dim, 0)


def sum_at_owner(x, axis, dim):
    pieces = split_up(x, dim, lax.axis_size(axis))
    arrived = lax.all_to_all(pieces, axis, split_axis=0, concat_axis=0, tiled=True)
    return arrived.astype(jnp.float32).sum(axis=0)


def over_copies(x, axis):
    everything = copy_for_each(x, axis)
    return jnp.sum(everything, axis=0)


def packed_total(arrays, axis):
    ends = [0]
    for a in arrays:
        ends.append(ends[-1] + a.size)
    subtotal = over_copies(jnp.concatenate([a.ravel() for a in arrays]), axis)
    return tuple((subtotal[b:e].reshape(a.shape) for a, b, e in zip(arrays, ends, ends[1:])))


def rotate(values, positions):
    half = values.shape[-1] // 2
    freqs = THETA ** (-jnp.arange(half, dtype=jnp.float32) / half)
    angles = positions.astype(jnp.float32)[:, None] * freqs[None, :]
    shape = (angles.shape[0],) + (1,) * (values.ndim - 2) + (half,)
    cosine = jnp.cos(angles).reshape(shape)
    sine = jnp.sin(angles).reshape(shape)
    first = values[..., :half]
    second = values[..., half:]
    return jnp.concatenate(
        [first * cosine - second * sine, second * cosine + first * sine], axis=-1
    )


def norm_rows(summed, gain):
    mean = jnp.mean(summed, axis=-1, keepdims=True)
    center = summed - mean
    spread = jnp.mean(center * center, axis=-1, keepdims=True)
    return center * lax.rsqrt(spread + EPS) * gain


def scaled_part(summed, sums, squares, width, gain):
    mean = sums / width
    spread = squares / width - mean * mean
    return (summed - mean[:, None]) * lax.rsqrt(spread + EPS)[:, None] * gain


def choose_slots(routes_block, experts, capacity):
    flat = routes_block.reshape(-1)
    onehot = (flat[:, None] == jnp.arange(experts, dtype=jnp.int32)[None, :]).astype(jnp.int32)
    before = jnp.cumsum(onehot, axis=0) - onehot
    slot = jnp.sum(before * onehot, axis=1)
    target = flat * capacity + slot
    return target[:, None] == jnp.arange(experts * capacity, dtype=jnp.int32)[None, :]


def body(
    tokens,
    lengths,
    key_cache,
    value_cache,
    query_weight,
    key_weight,
    value_weight,
    lambdas,
    head_gain,
    output_weight,
    norm1_gain,
    routes,
    route_logits,
    gate_weight,
    up_weight,
    down_weight,
    norm2_gain,
):
    bf16 = jnp.bfloat16
    f32 = jnp.float32
    tp_count = lax.axis_size("tp")
    tp_rank = lax.axis_index("tp")
    own, width = tokens.shape
    group = own * tp_count
    part = width // tp_count
    heads = lambdas.shape[0]
    head_dim = key_weight.shape[1] // 2
    length = key_cache.shape[1]
    group_rows = gathered_copies(tokens, "tp", 0)
    query = jnp.dot(group_rows, query_weight, preferred_element_type=f32).reshape(
        group, -1, 2, head_dim
    )
    query = rotate(query, lengths).astype(bf16).reshape(group, -1)
    query = lax.all_to_all(query, "tp", split_axis=0, concat_axis=1, tiled=True).reshape(
        own, heads, 2, head_dim
    )
    own_lengths = lax.dynamic_slice_in_dim(lengths, tp_rank * own, own)
    new_key = jnp.dot(tokens, key_weight, preferred_element_type=f32).reshape(own, 2, head_dim)
    new_key = rotate(new_key, own_lengths).astype(bf16)
    new_value = jnp.dot(tokens, value_weight, preferred_element_type=f32).astype(bf16)
    keys = key_cache.reshape(own, length, 2, head_dim)
    scale = head_dim ** (-0.5)
    past = jnp.einsum("bhmd,bjmd->bhmj", query, keys, preferred_element_type=f32) * scale
    live = jnp.arange(length, dtype=jnp.int32)[None, :] < own_lengths[:, None]
    past = jnp.where(live[:, None, None, :], past, -jnp.inf)
    selfs = jnp.einsum("bhmd,bmd->bhm", query, new_key, preferred_element_type=f32) * scale
    top = jnp.maximum(jnp.max(past, axis=-1), selfs)
    past_exp = jnp.exp(past - top[..., None])
    self_exp = jnp.exp(selfs - top)
    total = jnp.sum(past_exp, axis=-1) + self_exp
    past_prob = past_exp / total[..., None]
    self_prob = self_exp / total
    mixing = lambdas[None, :]
    past_weight = (past_prob[:, :, 0] - mixing[..., None] * past_prob[:, :, 1]).astype(bf16)
    self_weight = (self_prob[:, :, 0] - mixing * self_prob[:, :, 1]).astype(bf16)
    head_out = jnp.einsum("bhj,bje->bhe", past_weight, value_cache, preferred_element_type=f32)
    head_out = head_out + self_weight.astype(f32)[..., None] * new_value.astype(f32)[:, None, :]
    normed = (
        head_out
        * lax.rsqrt(jnp.mean(head_out * head_out, axis=-1, keepdims=True) + EPS)
        * head_gain
    )
    attended = normed.astype(bf16).reshape(own, -1)
    mix = jnp.dot(gathered_copies(attended, "tp", 0), output_weight, preferred_element_type=f32)
    column_start = tp_rank * part
    own_columns = lax.dynamic_slice_in_dim(group_rows, column_start, part, 1).astype(f32)
    summed = ALPHA * own_columns + mix
    whole = gathered_copies(summed, "tp", 1)
    settled = norm_rows(whole, norm1_gain).astype(bf16)
    settled_part = lax.dynamic_slice_in_dim(settled, column_start, part, 1)
    experts = lax.axis_size("ep")
    topk = routes.shape[1]
    capacity = min(group, max(2, 2 * group * topk // experts))
    chosen = choose_slots(routes, experts, capacity)
    placing = jnp.sum(chosen.reshape(group, topk, -1).astype(f32), axis=1).astype(bf16)
    route_weight = jax.nn.softmax(route_logits, axis=-1)
    gate_local = gate_weight[0]
    up_local = up_weight[0]
    down_local = down_weight[0]
    outgoing = lax.dot_general(
        placing, settled, (((0,), (0,)), ((), ())), preferred_element_type=f32
    )
    outgoing = outgoing.astype(bf16).reshape(experts, capacity, width)
    rows = lax.all_to_all(outgoing, "ep", split_axis=0, concat_axis=0, tiled=True)
    gate_h = jnp.einsum("scd,df->scf", rows, gate_local, preferred_element_type=f32)
    up_h = jnp.einsum("scd,df->scf", rows, up_local, preferred_element_type=f32)
    clipped = jnp.minimum(gate_h, LIMIT)
    linear = jnp.clip(up_h, -LIMIT, LIMIT)
    act = (clipped * jax.nn.sigmoid(SLOPE * clipped) * (linear + 1.0)).astype(bf16)
    terms = jnp.einsum("scf,fd->scd", act, down_local, preferred_element_type=f32)
    answers = sum_at_owner(terms.astype(jnp.bfloat16), "tp", 2).astype(bf16)
    selector = chosen.astype(bf16)
    back = lax.all_to_all(answers, "ep", split_axis=0, concat_axis=0, tiled=True)
    picked = jnp.dot(selector, back.reshape(experts * capacity, -1), preferred_element_type=f32)
    routed = jnp.sum(picked.reshape(group, topk, -1) * route_weight[:, :, None], axis=1)
    final = ALPHA * settled_part.astype(f32) + routed
    sums, squares = packed_total((jnp.sum(final, axis=1), jnp.sum(final * final, axis=1)), "tp")
    gain_part = lax.dynamic_slice_in_dim(norm2_gain, column_start, part)
    result = scaled_part(final, sums, squares, width, gain_part).astype(bf16)
    return result


def solution(mesh):
    in_specs = (
        P(("ep", "tp"), None),
        P("ep"),
        P(("ep", "tp"), None, None),
        P(("ep", "tp"), None, None),
        P(None, "tp"),
        P(),
        P(),
        P(),
        P(),
        P(None, "tp"),
        P(),
        P("ep", None),
        P("ep", None),
        P("ep", None, "tp"),
        P("ep", None, "tp"),
        P("ep", "tp", None),
        P(),
    )
    out_specs = P("ep", "tp")
    return jax.shard_map(body, mesh=mesh, in_specs=in_specs, out_specs=out_specs, check_vma=False)
```

profile of v0, /device:TPU:1, one launch (start us, length us, event | category | flops | bytes accessed | tf_op | source)
XLA Modules:
  0.0 130.2 jit_solution(14348994020305583358)
XLA Ops:
  0.0 1.5 %broadcast_in_dim.22 = bf16[4,4,1024]{2,1,0:T(4,128)(2,1)} broadcast(bf16[4,1024]{1,0:T(4,128)(2,1)} %param.17), dimensions={1,2} | broadcast | bytes 40960 | tf_op jit(solution)/shard_map/broadcast_in_dim | solution.py:15
  1.5 4.8 %all-to-all-start = ((bf16[4,4,1024]{2,1,0:T(4,128)(2,1)}), bf16[4,4,1024]{2,1,0:T(4,128)(2,1)S(1)}, u32[]{:S(2)}, u32[]{:S(2)}) async-start(bf16[4,4,1024]{2,1,0:T(4,128)(2,1)} %broadcast_in_dim.22), calls=%async_computation | async-start | bytes 65536 | tf_op jit(solution)/shard_map/all_to_all | solution.py:15
  7.0 0.7 fusion.54
  7.7 1.1 fusion.56
  9.2 0.8 fusion.6
  10.1 0.8 copy.109
  11.4 1.1 copy.102
  13.6 4.2 %all-to-all-start.1 = ((bf16[4,4,128]{2,1,0:T(4,128)(2,1)}), bf16[4,4,128]{2,1,0:T(4,128)(2,1)S(1)}, u32[]{:S(2)}, u32[]{:S(2)}) async-start(bf16[4,4,128]{2,1,0:T(4,128)(2,1)} %convert_element_type.68), calls=%async_computation.1 | async-start | bytes 8192 | tf_op jit(solution)/shard_map/all_to_all | solution.py:124
  18.6 3.4 %all-to-all-done.1 = bf16[4,4,128]{2,1,0:T(4,128)(2,1)S(1)} async-done(((bf16[4,4,128]{2,1,0:T(4,128)(2,1)}), bf16[4,4,128]{2,1,0:T(4,128)(2,1)S(1)}, u32[]{:S(2)}, u32[]{:S(2)}) %all-to-all-start.1) | async-done | bytes 4128 | tf_op jit(solution)/shard_map/all_to_all | solution.py:124
  25.4 3.4 %all-to-all-start.2 = ((bf16[4,4,512]{2,1,0:T(4,128)(2,1)}), bf16[4,4,512]{2,1,0:T(4,128)(2,1)S(1)}, u32[]{:S(2)}, u32[]{:S(2)}) async-start(bf16[4,4,512]{2,1,0:T(4,128)(2,1)} %broadcast_in_dim.26), calls=%async_computation.2 | async-start | bytes 32768 | tf_op jit(solution)/shard_map/all_to_all | solution.py:15
  28.8 4.1 %all-to-all-done.2 = bf16[4,4,512]{2,1,0:T(4,128)(2,1)S(1)} async-done(((bf16[4,4,512]{2,1,0:T(4,128)(2,1)}), bf16[4,4,512]{2,1,0:T(4,128)(2,1)S(1)}, u32[]{:S(2)}, u32[]{:S(2)}) %all-to-all-start.2) | async-done | bytes 16416 | tf_op jit(solution)/shard_map/all_to_all | solution.py:15
  33.7 3.3 %all-to-all-start.3 = ((f32[4,16,256]{2,1,0:T(8,128)}), f32[4,16,256]{2,1,0:T(8,128)S(1)}, u32[]{:S(2)}, u32[]{:S(2)}) async-start(f32[4,16,256]{2,1,0:T(8,128)} %broadcast_in_dim.27), calls=%async_computation.3 | async-start | bytes 131072 | tf_op jit(solution)/shard_map/all_to_all | solution.py:15
  37.1 4.4 %all-to-all-done.3 = f32[4,16,256]{2,1,0:T(8,128)S(1)} async-done(((f32[4,16,256]{2,1,0:T(8,128)}), f32[4,16,256]{2,1,0:T(8,128)S(1)}, u32[]{:S(2)}, u32[]{:S(2)}) %all-to-all-start.3) | async-done | bytes 65568 | tf_op jit(solution)/shard_map/all_to_all | solution.py:15
  43.1 42.4 %all_to_all.49 = bf16[128,2,1024]{2,1,0:T(2,128)(2,1)S(1)} all-to-all(bf16[128,2,1024]{2,1,0:T(2,128)(2,1)S(1)} %reshape.272), channel_id=1, replica_groups=mesh['ep'=128,'tp'=4] {'ep'}, dimensions={0} | all-to-all | bytes 1048576 | tf_op jit(solution)/shard_map/all_to_all | solution.py:174
  86.7 0.7 convolution_convert_fusion
  87.4 0.8 copy.141
  88.2 3.6 %all-to-all-start.5 = ((bf16[4,128,2,256]{3,1,2,0:T(8,128)(2,1)}), bf16[4,128,2,256]{3,1,2,0:T(8,128)(2,1)S(1)}, u32[]{:S(2)}, u32[]{:S(2)}) async-start(bf16[4,128,2,256]{3,1,2,0:T(8,128)(2,1)} %bitcast.101), calls=%async_computation.5 | async-start | bytes 1048576 | tf_op jit(solution)/shard_map/all_to_all | solution.py:37
  91.9 9.8 %all-to-all-done.5 = bf16[4,128,2,256]{3,1,2,0:T(8,128)(2,1)S(1)} async-done(((bf16[4,128,2,256]{3,1,2,0:T(8,128)(2,1)}), bf16[4,128,2,256]{3,1,2,0:T(8,128)(2,1)S(1)}, u32[]{:S(2)}, u32[]{:S(2)}) %all-to-all-start.5) | async-done | bytes 524320 | tf_op jit(solution)/shard_map/all_to_all | solution.py:37
  101.7 0.8 copy.115
  102.5 5.8 %all-to-all-start.6 = ((bf16[128,2,256]{2,1,0:T(2,128)(2,1)}), bf16[128,2,256]{2,1,0:T(2,128)(2,1)S(1)}, u32[]{:S(2)}, u32[]{:S(2)}) async-start(bf16[128,2,256]{2,1,0:T(2,128)(2,1)} %copy.115), calls=%async_computation.6 | async-start | bytes 262144 | tf_op jit(solution)/shard_map/all_to_all | solution.py:183
  108.3 12.8 %all-to-all-done.6 = bf16[128,2,256]{2,1,0:T(2,128)(2,1)S(1)} async-done(((bf16[128,2,256]{2,1,0:T(2,128)(2,1)}), bf16[128,2,256]{2,1,0:T(2,128)(2,1)S(1)}, u32[]{:S(2)}, u32[]{:S(2)}) %all-to-all-start.6) | async-done | bytes 131104 | tf_op jit(solution)/shard_map/all_to_all | solution.py:183
  122.2 3.2 %all-to-all-start.7 = ((f32[4,1,32]{2,1,0:T(1,128)}), f32[4,1,32]{2,1,0:T(1,128)S(1)}, u32[]{:S(2)}, u32[]{:S(2)}) async-start(f32[4,1,32]{2,1,0:T(1,128)} %broadcast_in_dim.28), calls=%async_computation.7 | async-start | bytes 4096 | tf_op jit(solution)/shard_map/all_to_all | solution.py:15
  125.4 0.8 dynamic_slice.15
  126.2 3.3 %all-to-all-done.7 = f32[4,1,32]{2,1,0:T(1,128)S(1)} async-done(((f32[4,1,32]{2,1,0:T(1,128)}), f32[4,1,32]{2,1,0:T(1,128)S(1)}, u32[]{:S(2)}, u32[]{:S(2)}) %all-to-all-start.7) | async-done | bytes 544 | tf_op jit(solution)/shard_map/all_to_all | solution.py:15
  (86 shorter events, 12.4 us)
Async XLA Ops:
  0.0 23.6 %copy-start = (bf16[4,1024,128]{2,1,0:T(8,128)(2,1)S(1)}, bf16[4,1024,128]{2,1,0:T(8,128)(2,1)}, u32[]{:S(2)}) copy-start(bf16[4,1024,128]{2,1,0:T(8,128)(2,1)} %param.20) | copy-start | bytes 3145732
  0.0 9.2 %copy-start.3 = (bf16[1024,128]{1,0:T(8,128)(2,1)S(1)}, bf16[1024,128]{1,0:T(8,128)(2,1)}, u32[]{:S(2)}) copy-start(bf16[1024,128]{1,0:T(8,128)(2,1)} %param.23) | copy-start | bytes 786436
  0.0 17.9 %copy-start.1 = (bf16[4,1024,128]{2,1,0:T(8,128)(2,1)S(1)}, bf16[4,1024,128]{2,1,0:T(8,128)(2,1)}, u32[]{:S(2)}) copy-start(bf16[4,1024,128]{2,1,0:T(8,128)(2,1)} %param.19) | copy-start | bytes 3145732
  1.5 11.0 %all-to-all-start = ((bf16[4,4,1024]{2,1,0:T(4,128)(2,1)}), bf16[4,4,1024]{2,1,0:T(4,128)(2,1)S(1)}, u32[]{:S(2)}, u32[]{:S(2)}) async-start(bf16[4,4,1024]{2,1,0:T(4,128)(2,1)} %broadcast_in_dim.22), calls=%async_computation | async-start | bytes 65536 | tf_op jit(solution)/shard_map/all_to_all | solution.py:15
  13.6 8.4 %all-to-all-start.1 = ((bf16[4,4,128]{2,1,0:T(4,128)(2,1)}), bf16[4,4,128]{2,1,0:T(4,128)(2,1)S(1)}, u32[]{:S(2)}, u32[]{:S(2)}) async-start(bf16[4,4,128]{2,1,0:T(4,128)(2,1)} %convert_element_type.68), calls=%async_computation.1 | async-start | bytes 8192 | tf_op jit(solution)/shard_map/all_to_all | solution.py:124
  22.9 0.7 copy-start.7
  23.6 9.3 %copy-start.2 = (bf16[512,256]{1,0:T(8,128)(2,1)S(1)}, bf16[512,256]{1,0:T(8,128)(2,1)}, u32[]{:S(2)}) copy-start(bf16[512,256]{1,0:T(8,128)(2,1)} %param.26) | copy-start | bytes 786436
  24.0 0.7 copy-start.8
  25.3 3.4 %copy-start.5 = (s32[16,6]{0,1:T(8,128)S(1)}, s32[16,6]{0,1:T(8,128)}, u32[]{:S(2)}) copy-start(s32[16,6]{0,1:T(8,128)} %param.28) | copy-start | bytes 1156
  25.4 7.6 %all-to-all-start.2 = ((bf16[4,4,512]{2,1,0:T(4,128)(2,1)}), bf16[4,4,512]{2,1,0:T(4,128)(2,1)S(1)}, u32[]{:S(2)}, u32[]{:S(2)}) async-start(bf16[4,4,512]{2,1,0:T(4,128)(2,1)} %broadcast_in_dim.26), calls=%async_computation.2 | async-start | bytes 32768 | tf_op jit(solution)/shard_map/all_to_all | solution.py:15
  33.7 7.7 %all-to-all-start.3 = ((f32[4,16,256]{2,1,0:T(8,128)}), f32[4,16,256]{2,1,0:T(8,128)S(1)}, u32[]{:S(2)}, u32[]{:S(2)}) async-start(f32[4,16,256]{2,1,0:T(8,128)} %broadcast_in_dim.27), calls=%async_computation.3 | async-start | bytes 131072 | tf_op jit(solution)/shard_map/all_to_all | solution.py:15
  41.8 0.7 copy-start.6
  43.1 42.4 %copy-start.9 = (bf16[1,1024,256]{2,1,0:T(8,128)(2,1)S(1)}, bf16[1,1024,256]{2,1,0:T(8,128)(2,1)}, u32[]{:S(2)}) copy-start(bf16[1,1024,256]{2,1,0:T(8,128)(2,1)} %param.30) | copy-start | bytes 1572868
  85.5 1.0 copy-start.10
  85.5 1.2 copy-start.11
  88.2 3.6 %copy-start.4 = (f32[16,6]{0,1:T(8,128)S(1)}, f32[16,6]{0,1:T(8,128)}, u32[]{:S(2)}) copy-start(f32[16,6]{0,1:T(8,128)} %param.29) | copy-start | bytes 1156
  88.2 13.4 %all-to-all-start.5 = ((bf16[4,128,2,256]{3,1,2,0:T(8,128)(2,1)}), bf16[4,128,2,256]{3,1,2,0:T(8,128)(2,1)S(1)}, u32[]{:S(2)}, u32[]{:S(2)}) async-start(bf16[4,128,2,256]{3,1,2,0:T(8,128)(2,1)} %bitcast.101), calls=%async_computation.5 | async-start | bytes 1048576 | tf_op jit(solution)/shard_map/all_to_all | solution.py:37
  102.5 18.6 %all-to-all-start.6 = ((bf16[128,2,256]{2,1,0:T(2,128)(2,1)}), bf16[128,2,256]{2,1,0:T(2,128)(2,1)S(1)}, u32[]{:S(2)}, u32[]{:S(2)}) async-start(bf16[128,2,256]{2,1,0:T(2,128)(2,1)} %copy.115), calls=%async_computation.6 | async-start | bytes 262144 | tf_op jit(solution)/shard_map/all_to_all | solution.py:183
  122.2 7.3 %all-to-all-start.7 = ((f32[4,1,32]{2,1,0:T(1,128)}), f32[4,1,32]{2,1,0:T(1,128)S(1)}, u32[]{:S(2)}, u32[]{:S(2)}) async-start(f32[4,1,32]{2,1,0:T(1,128)} %broadcast_in_dim.28), calls=%async_computation.7 | async-start | bytes 4096 | tf_op jit(solution)/shard_map/all_to_all | solution.py:15
where the time goes:
time: 131 us; the launch traced here: 130 us
  blocking collectives  42.4 us (32%)
  waiting for transfers between devices  37.7 us (29%)
  starting transfers between devices  28.3 us (22%)
  local copies, waits for them, and re-layouts  12.4 us (9%)
  matrix products  4.71 us (4%)
  other arithmetic  4.47 us (3%)
    all_to_all x1, blocking collectives, body(): lax.all_to_all(outgoing, 'ep', split_axis=0, concat_axis=0, tiled=True)  42.4 us
    all_to_all x4, starting transfers between devices, copy_for_each(): lax.all_to_all(jnp.broadcast_to(x[None], (count, *x.shape)), axis, 0, 0,...  14.7 us
    all_to_all x1, waiting for transfers between devices, body(): lax.all_to_all(answers, 'ep', split_axis=0, concat_axis=0, tiled=True)  12.8 us
    all_to_all x4, waiting for transfers between devices, copy_for_each(): lax.all_to_all(jnp.broadcast_to(x[None], (count, *x.shape)), axis, 0, 0,...  11.7 us
    all_to_all x1, waiting for transfers between devices, sum_at_owner(): lax.all_to_all(pieces, axis, split_axis=0, concat_axis=0, tiled=True)  9.76 us
    all_to_all x1, starting transfers between devices, body(): lax.all_to_all(answers, 'ep', split_axis=0, concat_axis=0, tiled=True)  5.77 us
    unnamed x28, local copies, waits for them, and re-layouts  5.31 us
    all_to_all x1, starting transfers between devices, body(): lax.all_to_all(query, 'tp', split_axis=0, concat_axis=1, tiled=True)  4.23 us
  transfers between devices with their start and end apart: 7, of which 6 were waited for; matrix products, arithmetic and copies ran while one was open for 6% of the time, Pallas kernels for 0%

commit v1 on v0

--- a/solution.py
+++ b/solution.py
@@ -121,9 +121,16 @@
         group, -1, 2, head_dim
     )
     query = rotate(query, lengths).astype(bf16).reshape(group, -1)
-    query = lax.all_to_all(query, "tp", split_axis=0, concat_axis=1, tiled=True).reshape(
-        own, heads, 2, head_dim
-    )
+    expand_the_ports = lambda load: jnp.concatenate(
+        lax.all_to_all(
+            jnp.stack(jnp.split(load, lax.axis_size("tp"), 0), 0),
+            axis_name="tp",
+            split_axis=0,
+            concat_axis=0,
+        ),
+        1,
+    )
+    query = expand_the_ports(query).reshape(own, heads, 2, head_dim)
     own_lengths = lax.dynamic_slice_in_dim(lengths, tp_rank * own, own)
     new_key = jnp.dot(tokens, key_weight, preferred_element_type=f32).reshape(own, 2, head_dim)
     new_key = rotate(new_key, own_lengths).astype(bf16)

time: 131 us -> 131 us (level)
  no operation moved by 1% of the time
where the time goes in v1:
time: 131 us; the launch traced here: 130 us
  blocking collectives  42.4 us (32%)
  waiting for transfers between devices  37.7 us (29%)
  starting transfers between devices  28.3 us (22%)
  local copies, waits for them, and re-layouts  12 us (9%)
  other arithmetic  5.08 us (4%)
  matrix products  4.72 us (4%)
    all_to_all x1, blocking collectives, body(): lax.all_to_all(outgoing, 'ep', split_axis=0, concat_axis=0, tiled=True)  42.4 us
    all_to_all x4, starting transfers between devices, copy_for_each(): lax.all_to_all(jnp.broadcast_to(x[None], (count, *x.shape)), axis, 0, 0,...  14.7 us
    all_to_all x1, waiting for transfers between devices, body(): lax.all_to_all(answers, 'ep', split_axis=0, concat_axis=0, tiled=True)  12.8 us
    all_to_all x4, waiting for transfers between devices, copy_for_each(): lax.all_to_all(jnp.broadcast_to(x[None], (count, *x.shape)), axis, 0, 0,...  11.7 us
    all_to_all x1, waiting for transfers between devices, sum_at_owner(): lax.all_to_all(pieces, axis, split_axis=0, concat_axis=0, tiled=True)  9.76 us
    all_to_all x1, starting transfers between devices, body(): lax.all_to_all(answers, 'ep', split_axis=0, concat_axis=0, tiled=True)  5.77 us
    unnamed x28, local copies, waits for them, and re-layouts  5.31 us
    all_to_all x1, starting transfers between devices, body(): lax.all_to_all(jnp.stack(jnp.split(load, lax.axis_size('tp'), 0), 0), axi...  4.24 us
  transfers between devices with their start and end apart: 7, of which 6 were waited for; matrix products, arithmetic and copies ran while one was open for 6% of the time, Pallas kernels for 0%

profile of v1, /device:TPU:1, one launch (start us, length us, event | category | flops | bytes accessed | tf_op | source)
XLA Modules:
  0.0 130.5 jit_solution(17092558044857435666)
XLA Ops:
  0.0 1.5 %broadcast_in_dim.22 = bf16[4,4,1024]{2,1,0:T(4,128)(2,1)} broadcast(bf16[4,1024]{1,0:T(4,128)(2,1)} %param.17), dimensions={1,2} | broadcast | bytes 40960 | tf_op jit(solution)/shard_map/broadcast_in_dim | solution.py:15
  1.5 4.8 %all-to-all-start = ((bf16[4,4,1024]{2,1,0:T(4,128)(2,1)}), bf16[4,4,1024]{2,1,0:T(4,128)(2,1)S(1)}, u32[]{:S(2)}, u32[]{:S(2)}) async-start(bf16[4,4,1024]{2,1,0:T(4,128)(2,1)} %broadcast_in_dim.22), calls=%async_computation | async-start | bytes 65536 | tf_op jit(solution)/shard_map/all_to_all | solution.py:15
  7.0 0.7 fusion.57
  7.9 1.1 fusion.59
  9.2 0.8 fusion.6
  10.1 0.8 copy.127
  11.4 1.1 copy.117
  13.9 4.2 %all-to-all-start.1 = ((bf16[4,4,128]{2,1,0:T(4,128)(2,1)}), bf16[4,4,128]{2,1,0:T(4,128)(2,1)S(1)}, u32[]{:S(2)}, u32[]{:S(2)}) async-start(bf16[4,4,128]{2,1,0:T(4,128)(2,1)} %pad_maximum_fusion), calls=%async_computation.1 | async-start | bytes 8192 | tf_op jit(solution)/shard_map/all_to_all | solution.py:125
  18.9 3.4 %all-to-all-done.1 = bf16[4,4,128]{2,1,0:T(4,128)(2,1)S(1)} async-done(((bf16[4,4,128]{2,1,0:T(4,128)(2,1)}), bf16[4,4,128]{2,1,0:T(4,128)(2,1)S(1)}, u32[]{:S(2)}, u32[]{:S(2)}) %all-to-all-start.1) | async-done | bytes 4128 | tf_op jit(solution)/shard_map/all_to_all | solution.py:125
  25.6 3.4 %all-to-all-start.2 = ((bf16[4,4,512]{2,1,0:T(4,128)(2,1)}), bf16[4,4,512]{2,1,0:T(4,128)(2,1)S(1)}, u32[]{:S(2)}, u32[]{:S(2)}) async-start(bf16[4,4,512]{2,1,0:T(4,128)(2,1)} %broadcast_in_dim.26), calls=%async_computation.2 | async-start | bytes 32768 | tf_op jit(solution)/shard_map/all_to_all | solution.py:15
  29.1 4.1 %all-to-all-done.2 = bf16[4,4,512]{2,1,0:T(4,128)(2,1)S(1)} async-done(((bf16[4,4,512]{2,1,0:T(4,128)(2,1)}), bf16[4,4,512]{2,1,0:T(4,128)(2,1)S(1)}, u32[]{:S(2)}, u32[]{:S(2)}) %all-to-all-start.2) | async-done | bytes 16416 | tf_op jit(solution)/shard_map/all_to_all | solution.py:15
  34.0 3.3 %all-to-all-start.3 = ((f32[4,16,256]{2,1,0:T(8,128)}), f32[4,16,256]{2,1,0:T(8,128)S(1)}, u32[]{:S(2)}, u32[]{:S(2)}) async-start(f32[4,16,256]{2,1,0:T(8,128)} %broadcast_in_dim.27), calls=%async_computation.3 | async-start | bytes 131072 | tf_op jit(solution)/shard_map/all_to_all | solution.py:15
  37.4 4.4 %all-to-all-done.3 = f32[4,16,256]{2,1,0:T(8,128)S(1)} async-done(((f32[4,16,256]{2,1,0:T(8,128)}), f32[4,16,256]{2,1,0:T(8,128)S(1)}, u32[]{:S(2)}, u32[]{:S(2)}) %all-to-all-start.3) | async-done | bytes 65568 | tf_op jit(solution)/shard_map/all_to_all | solution.py:15
  43.4 42.4 %all_to_all.41 = bf16[128,2,1024]{2,1,0:T(2,128)(2,1)S(1)} all-to-all(bf16[128,2,1024]{2,1,0:T(2,128)(2,1)S(1)} %reshape.294), channel_id=1, replica_groups=mesh['ep'=128,'tp'=4] {'ep'}, dimensions={0} | all-to-all | bytes 1048576 | tf_op jit(solution)/shard_map/all_to_all | solution.py:181
  86.9 0.7 convolution_convert_fusion
  87.7 0.8 copy.159
  88.5 3.6 %all-to-all-start.5 = ((bf16[4,128,2,256]{3,1,2,0:T(8,128)(2,1)}), bf16[4,128,2,256]{3,1,2,0:T(8,128)(2,1)S(1)}, u32[]{:S(2)}, u32[]{:S(2)}) async-start(bf16[4,128,2,256]{3,1,2,0:T(8,128)(2,1)} %bitcast.107), calls=%async_computation.5 | async-start | bytes 1048576 | tf_op jit(solution)/shard_map/all_to_all | solution.py:37
  92.2 9.8 %all-to-all-done.5 = bf16[4,128,2,256]{3,1,2,0:T(8,128)(2,1)S(1)} async-done(((bf16[4,128,2,256]{3,1,2,0:T(8,128)(2,1)}), bf16[4,128,2,256]{3,1,2,0:T(8,128)(2,1)S(1)}, u32[]{:S(2)}, u32[]{:S(2)}) %all-to-all-start.5) | async-done | bytes 524320 | tf_op jit(solution)/shard_map/all_to_all | solution.py:37
  102.0 0.8 copy.133
  102.8 5.8 %all-to-all-start.6 = ((bf16[128,2,256]{2,1,0:T(2,128)(2,1)}), bf16[128,2,256]{2,1,0:T(2,128)(2,1)S(1)}, u32[]{:S(2)}, u32[]{:S(2)}) async-start(bf16[128,2,256]{2,1,0:T(2,128)(2,1)} %copy.133), calls=%async_computation.6 | async-start | bytes 262144 | tf_op jit(solution)/shard_map/all_to_all | solution.py:190
  108.6 12.8 %all-to-all-done.6 = bf16[128,2,256]{2,1,0:T(2,128)(2,1)S(1)} async-done(((bf16[128,2,256]{2,1,0:T(2,128)(2,1)}), bf16[128,2,256]{2,1,0:T(2,128)(2,1)S(1)}, u32[]{:S(2)}, u32[]{:S(2)}) %all-to-all-start.6) | async-done | bytes 131104 | tf_op jit(solution)/shard_map/all_to_all | solution.py:190
  122.4 3.2 %all-to-all-start.7 = ((f32[4,1,32]{2,1,0:T(1,128)}), f32[4,1,32]{2,1,0:T(1,128)S(1)}, u32[]{:S(2)}, u32[]{:S(2)}) async-start(f32[4,1,32]{2,1,0:T(1,128)} %broadcast_in_dim.28), calls=%async_computation.7 | async-start | bytes 4096 | tf_op jit(solution)/shard_map/all_to_all | solution.py:15
  125.7 0.8 dynamic_slice.15
  126.4 3.3 %all-to-all-done.7 = f32[4,1,32]{2,1,0:T(1,128)S(1)} async-done(((f32[4,1,32]{2,1,0:T(1,128)}), f32[4,1,32]{2,1,0:T(1,128)S(1)}, u32[]{:S(2)}, u32[]{:S(2)}) %all-to-all-start.7) | async-done | bytes 544 | tf_op jit(solution)/shard_map/all_to_all | solution.py:15
  (93 shorter events, 12.7 us)
Async XLA Ops:
  0.0 23.9 %copy-start = (bf16[4,1024,128]{2,1,0:T(8,128)(2,1)S(1)}, bf16[4,1024,128]{2,1,0:T(8,128)(2,1)}, u32[]{:S(2)}) copy-start(bf16[4,1024,128]{2,1,0:T(8,128)(2,1)} %param.20) | copy-start | bytes 3145732
  0.0 9.2 %copy-start.3 = (bf16[1024,128]{1,0:T(8,128)(2,1)S(1)}, bf16[1024,128]{1,0:T(8,128)(2,1)}, u32[]{:S(2)}) copy-start(bf16[1024,128]{1,0:T(8,128)(2,1)} %param.23) | copy-start | bytes 786436
  0.0 18.2 %copy-start.1 = (bf16[4,1024,128]{2,1,0:T(8,128)(2,1)S(1)}, bf16[4,1024,128]{2,1,0:T(8,128)(2,1)}, u32[]{:S(2)}) copy-start(bf16[4,1024,128]{2,1,0:T(8,128)(2,1)} %param.19) | copy-start | bytes 3145732
  1.5 11.0 %all-to-all-start = ((bf16[4,4,1024]{2,1,0:T(4,128)(2,1)}), bf16[4,4,1024]{2,1,0:T(4,128)(2,1)S(1)}, u32[]{:S(2)}, u32[]{:S(2)}) async-start(bf16[4,4,1024]{2,1,0:T(4,128)(2,1)} %broadcast_in_dim.22), calls=%async_computation | async-start | bytes 65536 | tf_op jit(solution)/shard_map/all_to_all | solution.py:15
  13.9 8.4 %all-to-all-start.1 = ((bf16[4,4,128]{2,1,0:T(4,128)(2,1)}), bf16[4,4,128]{2,1,0:T(4,128)(2,1)S(1)}, u32[]{:S(2)}, u32[]{:S(2)}) async-start(bf16[4,4,128]{2,1,0:T(4,128)(2,1)} %pad_maximum_fusion), calls=%async_computation.1 | async-start | bytes 8192 | tf_op jit(solution)/shard_map/all_to_all | solution.py:125
  23.2 0.7 copy-start.7
  23.9 9.3 %copy-start.2 = (bf16[512,256]{1,0:T(8,128)(2,1)S(1)}, bf16[512,256]{1,0:T(8,128)(2,1)}, u32[]{:S(2)}) copy-start(bf16[512,256]{1,0:T(8,128)(2,1)} %param.26) | copy-start | bytes 786436
  24.3 0.7 copy-start.8
  25.6 3.4 %copy-start.5 = (s32[16,6]{0,1:T(8,128)S(1)}, s32[16,6]{0,1:T(8,128)}, u32[]{:S(2)}) copy-start(s32[16,6]{0,1:T(8,128)} %param.28) | copy-start | bytes 1156
  25.6 7.6 %all-to-all-start.2 = ((bf16[4,4,512]{2,1,0:T(4,128)(2,1)}), bf16[4,4,512]{2,1,0:T(4,128)(2,1)S(1)}, u32[]{:S(2)}, u32[]{:S(2)}) async-start(bf16[4,4,512]{2,1,0:T(4,128)(2,1)} %broadcast_in_dim.26), calls=%async_computation.2 | async-start | bytes 32768 | tf_op jit(solution)/shard_map/all_to_all | solution.py:15
  34.0 7.7 %all-to-all-start.3 = ((f32[4,16,256]{2,1,0:T(8,128)}), f32[4,16,256]{2,1,0:T(8,128)S(1)}, u32[]{:S(2)}, u32[]{:S(2)}) async-start(f32[4,16,256]{2,1,0:T(8,128)} %broadcast_in_dim.27), calls=%async_computation.3 | async-start | bytes 131072 | tf_op jit(solution)/shard_map/all_to_all | solution.py:15
  42.1 0.7 copy-start.6
  43.4 42.4 %copy-start.9 = (bf16[1,1024,256]{2,1,0:T(8,128)(2,1)S(1)}, bf16[1,1024,256]{2,1,0:T(8,128)(2,1)}, u32[]{:S(2)}) copy-start(bf16[1,1024,256]{2,1,0:T(8,128)(2,1)} %param.30) | copy-start | bytes 1572868
  85.7 1.0 copy-start.10
  85.8 1.2 copy-start.11
  88.5 3.6 %copy-start.4 = (f32[16,6]{0,1:T(8,128)S(1)}, f32[16,6]{0,1:T(8,128)}, u32[]{:S(2)}) copy-start(f32[16,6]{0,1:T(8,128)} %param.29) | copy-start | bytes 1156
  88.5 13.4 %all-to-all-start.5 = ((bf16[4,128,2,256]{3,1,2,0:T(8,128)(2,1)}), bf16[4,128,2,256]{3,1,2,0:T(8,128)(2,1)S(1)}, u32[]{:S(2)}, u32[]{:S(2)}) async-start(bf16[4,128,2,256]{3,1,2,0:T(8,128)(2,1)} %bitcast.107), calls=%async_computation.5 | async-start | bytes 1048576 | tf_op jit(solution)/shard_map/all_to_all | solution.py:37
  102.8 18.6 %all-to-all-start.6 = ((bf16[128,2,256]{2,1,0:T(2,128)(2,1)}), bf16[128,2,256]{2,1,0:T(2,128)(2,1)S(1)}, u32[]{:S(2)}, u32[]{:S(2)}) async-start(bf16[128,2,256]{2,1,0:T(2,128)(2,1)} %copy.133), calls=%async_computation.6 | async-start | bytes 262144 | tf_op jit(solution)/shard_map/all_to_all | solution.py:190
  122.4 7.3 %all-to-all-start.7 = ((f32[4,1,32]{2,1,0:T(1,128)}), f32[4,1,32]{2,1,0:T(1,128)S(1)}, u32[]{:S(2)}, u32[]{:S(2)}) async-start(f32[4,1,32]{2,1,0:T(1,128)} %broadcast_in_dim.28), calls=%async_computation.7 | async-start | bytes 4096 | tf_op jit(solution)/shard_map/all_to_all | solution.py:15
